TPU v7x, 32 devices: a whole 2x2x4 slice. The times are simulated.
32 devices in a mesh: grp: 2 (over y), sp: 4 (over z), fs: 2 (over x), tp: 2 (over core).
Axes of the slice: x: 2, y: 2, z: 4, core: 2. Of those that a mesh axis runs over, the one named last changes fastest.
Arguments:
- tokens: bfloat16 [8, 512, 2048], P(('grp', 'fs'), ('sp', 'tp')), parts along dimension 0, may hold values from -24 to 24
- norm_gain: float32 [2048], replicated, may hold values from 0.1 to 1.9
- w_query: bfloat16 [2048, 1024], P(('sp', 'fs'), 'tp'), may hold values from -0.125 to 0.125
- w_key: bfloat16 [2048, 1024], P(('sp', 'fs'), 'tp'), may hold values from -0.125 to 0.125
- w_value: bfloat16 [2048, 1024], P(('sp', 'fs'), 'tp'), may hold values from -0.125 to 0.125
- query_gain: float32 [1024], P('tp'), may hold values from 1 to 26
- key_gain: float32 [1024], P('tp'), may hold values from 0.1 to 1.9
- mix_lambda: float32 [8], P('tp'), may hold values from 0.3 to 0.8
- head_gain: float32 [128], replicated, may hold values from 0.1 to 1.9
- w_gate_b: bfloat16 [2048, 1024], P(('sp', 'fs'), 'tp'), may hold values from -0.125 to 0.125
- w_gate_c: bfloat16 [2048, 1024], P(('sp', 'fs'), 'tp'), may hold values from -0.125 to 0.125
- w_conv_in: bfloat16 [2048, 1024], P(('sp', 'fs'), 'tp'), may hold values from -0.125 to 0.125
- conv_taps: float32 [3, 1024], P(None, 'tp'), may hold values from -3 to 3
- w_out_attn: bfloat16 [1024, 2048], P('tp', ('sp', 'fs')), may hold values from -0.125 to 0.125
- w_out_conv: bfloat16 [1024, 2048], P('tp', ('sp', 'fs')), may hold values from -0.125 to 0.125
Outputs:
- mixed: bfloat16 [8, 512, 2048], P(('grp', 'fs'), ('sp', 'tp')), parts along dimension 0
There are 2 independent parts, one for each index of `grp`. A program takes and returns all parts, laid end to end along the dimension named above; an argument that names none is the same for every part. Nothing has to cross between parts.
All inputs are finite; a program needn't handle non-finite values.
Results may differ from a plain program's by a relative error of at most 0.04.
Values may be sent and summed in bfloat16 or wider, within the bound.
No kernel may reach another device: no remote copies, remote signals or barrier semaphores. Data moves between devices by JAX's collectives and lax.ppermute only.
A program may use at most 128 MiB of HBM per device.

v0:
```python
import math

import jax
import jax.numpy as jnp
from jax import lax
from jax.sharding import PartitionSpec as P

DK = 64
DV = 128
KW = 3


EPS = 1e-06
NEG = -1e30
OUT_SCALE = 0.8


def from_behind(block, axis, distance):
    devices = range(lax.axis_size(axis))
    route = [(i - distance, i) for i in devices if i - distance in devices]
    return lax.ppermute(block, axis, route)


def rms_scale(values, gain):
    wide = values.astype(jnp.float32)
    return wide * lax.rsqrt(jnp.mean(wide * wide, axis=-1, keepdims=True) + EPS) * gain


def attend_heads(normed, wq_full, wk_full, wv_full, query_gain, key_gain, mix_lambda, head_gain):
    rows = normed.shape[0]
    heads_here = mix_lambda.shape[0]
    query = rms_scale(
        jnp.dot(normed, wq_full, preferred_element_type=jnp.float32)
        .astype(jnp.bfloat16)
        .reshape(rows, heads_here, 2, DK),
        query_gain.reshape(heads_here, 2, DK),
    ).astype(jnp.bfloat16)
    key = rms_scale(
        jnp.dot(normed, wk_full, preferred_element_type=jnp.float32)
        .astype(jnp.bfloat16)
        .reshape(rows, heads_here, 2, DK),
        key_gain.reshape(heads_here, 2, DK),
    ).astype(jnp.bfloat16)
    value = jnp.dot(normed, wv_full, preferred_element_type=jnp.float32).astype(jnp.bfloat16)
    q_pos = lax.axis_index("sp") * rows + jnp.arange(rows, dtype=jnp.int32)
    init = (
        jnp.full((heads_here, 2, rows), NEG, jnp.float32),
        jnp.zeros((heads_here, 2, rows), jnp.float32),
        jnp.zeros((heads_here, 2, rows, DV), jnp.float32),
    )
    key_piece = lax.all_gather(key.reshape(rows, heads_here * 2 * DK), "sp", axis=0, tiled=True)
    value_piece = lax.all_gather(value, "sp", axis=0, tiled=True)
    count = key_piece.shape[0]
    width = math.gcd(count, 1024)
    blocks = count // width
    key_blocks = key_piece.reshape(blocks, width, heads_here, 2, DK)
    value_blocks = value_piece.reshape(blocks, width, heads_here, DV)
    begins = jnp.arange(blocks, dtype=jnp.int32) * width

    def step(state, inputs):
        running, total, summed = state
        key_block, value_block, begin = inputs
        k_pos = begin + jnp.arange(width, dtype=jnp.int32)
        score = jnp.einsum(
            "qhmd,khmd->hmqk", query, key_block, preferred_element_type=jnp.float32
        ) * DK ** (-0.5)
        allowed = k_pos[None, :] <= q_pos[:, None]
        score = jnp.where(allowed, score, NEG)
        newest = jnp.maximum(running, jnp.max(score, axis=-1))
        factor = jnp.exp(running - newest)
        weights = jnp.where(allowed, jnp.exp(score - newest[..., None]), 0.0)
        total = total * factor + jnp.sum(weights, axis=-1)
        summed = summed * factor[..., None] + jnp.einsum(
            "hmqk,khd->hmqd",
            weights.astype(jnp.bfloat16),
            value_block,
            preferred_element_type=jnp.float32,
        )
        return ((newest, total, summed), None)

    result, unused = lax.scan(step, init, (key_blocks, value_blocks, begins))
    running, total, summed = result
    head_map = summed / total[..., None]
    differ = head_map[:, 0] - mix_lambda[:, None, None] * head_map[:, 1]
    normal = rms_scale(differ, head_gain) * OUT_SCALE
    return normal.transpose(1, 0, 2).reshape(rows, heads_here * DV).astype(jnp.bfloat16)


def gated_conv(normed, wb_full, wc_full, wi_full, conv_taps):
    rows = normed.shape[0]
    gate_b = jnp.dot(normed, wb_full, preferred_element_type=jnp.float32).astype(jnp.bfloat16)
    gate_c = jnp.dot(normed, wc_full, preferred_element_type=jnp.float32).astype(jnp.bfloat16)
    conv_in = jnp.dot(normed, wi_full, preferred_element_type=jnp.float32).astype(jnp.bfloat16)
    shaped = (gate_c.astype(jnp.float32) * conv_in.astype(jnp.float32)).astype(jnp.bfloat16)
    edge = from_behind(shaped[rows - (KW - 1) :], "sp", 1)
    padded = jnp.concatenate([edge, shaped], axis=0).astype(jnp.float32)
    conv = conv_taps[0][None, :] * padded[0:rows]
    for tap in range(1, KW):
        conv = conv + conv_taps[tap][None, :] * padded[tap : tap + rows]
    return (gate_b.astype(jnp.float32) * conv).astype(jnp.bfloat16)


def normalize_rows(own_rows, norm_gain):
    return rms_scale(lax.all_gather(own_rows, "tp", axis=0, tiled=True), norm_gain).astype(
        jnp.bfloat16
    )


def on_device(
    tokens,
    norm_gain,
    w_query,
    w_key,
    w_value,
    query_gain,
    key_gain,
    mix_lambda,
    head_gain,
    w_gate_b,
    w_gate_c,
    w_conv_in,
    conv_taps,
    w_out_attn,
    w_out_conv,
):
    seq_count = tokens.shape[0]
    gathered = (
        lax.all_gather(w_query, ("sp", "fs"), axis=0, tiled=True),
        lax.all_gather(w_key, ("sp", "fs"), axis=0, tiled=True),
        lax.all_gather(w_value, ("sp", "fs"), axis=0, tiled=True),
        lax.all_gather(w_gate_b, ("sp", "fs"), axis=0, tiled=True),
        lax.all_gather(w_gate_c, ("sp", "fs"), axis=0, tiled=True),
        lax.all_gather(w_conv_in, ("sp", "fs"), axis=0, tiled=True),
        lax.all_gather(w_out_attn, ("sp", "fs"), axis=1, tiled=True),
        lax.all_gather(w_out_conv, ("sp", "fs"), axis=1, tiled=True),
    )
    normed_list = [normalize_rows(tokens[index], norm_gain) for index in range(seq_count)]
    attn_list = [
        attend_heads(
            normed,
            gathered[0],
            gathered[1],
            gathered[2],
            query_gain,
            key_gain,
            mix_lambda,
            head_gain,
        )
        for normed in normed_list
    ]
    conv_list = [
        gated_conv(normed, gathered[3], gathered[4], gathered[5], conv_taps)
        for normed in normed_list
    ]
    out_attn = gathered[6]
    out_conv = gathered[7]
    results = []
    for index in range(seq_count):
        attn = attn_list[index]
        conv_out = conv_list[index]
        results.append(
            lax.psum_scatter(
                (
                    jnp.dot(attn, out_attn, preferred_element_type=jnp.float32)
                    + jnp.dot(conv_out, out_conv, preferred_element_type=jnp.float32)
                ).astype(jnp.bfloat16),
                "tp",
                scatter_dimension=0,
                tiled=True,
            )
        )
    return jnp.stack(results, axis=0)


def solution(mesh):
    placed = (
        P(("grp", "fs"), ("sp", "tp"), None),
        P(),
        P(("sp", "fs"), "tp"),
        P(("sp", "fs"), "tp"),
        P(("sp", "fs"), "tp"),
        P("tp"),
        P("tp"),
        P("tp"),
        P(),
        P(("sp", "fs"), "tp"),
        P(("sp", "fs"), "tp"),
        P(("sp", "fs"), "tp"),
        P(None, "tp"),
        P("tp", ("sp", "fs")),
        P("tp", ("sp", "fs")),
    )
    return jax.shard_map(
        on_device,
        mesh=mesh,
        in_specs=placed,
        out_specs=P(("grp", "fs"), ("sp", "tp"), None),
        check_vma=False,
    )
```

profile of v0, /device:TPU:0, one launch (start us, length us, event | category | flops | bytes accessed | tf_op | source)
XLA Modules:
  0.0 453.7 jit_solution(17097135816359609861)
XLA Ops:
  12.1 2.3 all-gather
  14.6 2.2 all-gather.1
  17.2 44.2 %all-gather.13.cloned.1.call-done = bf16[2048,512]{1,0:T(8,128)(2,1)} async-done(((bf16[256,512]{1,0:T(8,128)(2,1)}), bf16[2048,512]{1,0:T(8,128)(2,1)}) %all-gather.13.cloned.1.call-update) | async-done | bytes 2097168 | tf_op jit(solution)/shard_map/all_gather | solution.py:129
  61.4 3.0 fusion.86
  71.8 20.0 %all_gather.45 = bf16[512,512]{1,0:T(8,128)(2,1)S(1)} all-gather(bf16[128,512]{1,0:T(8,128)(2,1)S(1)} %get-tuple-element.69), channel_id=1, replica_groups=mesh['grp'=2,'sp'=4,'fs'=2,'tp'=2] {'sp'}, dimensions={0}, use_global_device_ids=true | all-gather | bytes 655360 | tf_op jit(solution)/shard_map/all_gather | solution.py:51
  92.8 24.1 %all-gather.11.cloned.1.call-done = bf16[2048,512]{1,0:T(8,128)(2,1)} async-done(((bf16[256,512]{1,0:T(8,128)(2,1)}), bf16[2048,512]{1,0:T(8,128)(2,1)}) %all-gather.11.cloned.1.call-update) | async-done | bytes 2097168 | tf_op jit(solution)/shard_map/all_gather | solution.py:128
  119.2 3.2 fusion.2
  122.4 20.8 %all_gather.54 = bf16[512,512]{1,0:T(8,128)(2,1)} all-gather(bf16[128,512]{1,0:T(8,128)(2,1)S(1)} %copy-done.11), channel_id=1, replica_groups=mesh['grp'=2,'sp'=4,'fs'=2,'tp'=2] {'sp'}, dimensions={0}, use_global_device_ids=true | all-gather | bytes 655360 | tf_op jit(solution)/shard_map/all_gather | solution.py:51
  145.9 3.0 fusion.4
  149.7 20.3 %all-gather.15.cloned.1.call-done = bf16[2048,512]{1,0:T(8,128)(2,1)} async-done(((bf16[256,512]{1,0:T(8,128)(2,1)}), bf16[2048,512]{1,0:T(8,128)(2,1)}) %all-gather.15.cloned.1.call-update) | async-done | bytes 2097168 | tf_op jit(solution)/shard_map/all_gather | solution.py:130
  170.0 2.1 convolution_convert_fusion.3
  172.1 19.2 %all_gather.55 = bf16[512,512]{1,0:T(8,128)(2,1)S(1)} all-gather(bf16[128,512]{1,0:T(8,128)(2,1)S(1)} %convolution_convert_fusion.3), channel_id=1, replica_groups=mesh['grp'=2,'sp'=4,'fs'=2,'tp'=2] {'sp'}, dimensions={0}, use_global_device_ids=true | all-gather | bytes 655360 | tf_op jit(solution)/shard_map/all_gather | solution.py:52
  191.5 2.1 convolution_convert_fusion.9
  193.6 18.4 %all_gather.47 = bf16[512,512]{1,0:T(8,128)(2,1)S(1)} all-gather(bf16[128,512]{1,0:T(8,128)(2,1)S(1)} %convolution_convert_fusion.9), channel_id=1, replica_groups=mesh['grp'=2,'sp'=4,'fs'=2,'tp'=2] {'sp'}, dimensions={0}, use_global_device_ids=true | all-gather | bytes 655360 | tf_op jit(solution)/shard_map/all_gather | solution.py:52
  213.0 8.9 %all-gather.21.cloned.1.call-done = bf16[2048,512]{1,0:T(8,128)(2,1)} async-done(((bf16[256,512]{1,0:T(8,128)(2,1)}), bf16[2048,512]{1,0:T(8,128)(2,1)}) %all-gather.21.cloned.1.call-update) | async-done | bytes 2097168 | tf_op jit(solution)/shard_map/all_gather | solution.py:132
  224.0 48.0 %all-gather.23.cloned.1.call-done = bf16[2048,512]{1,0:T(8,128)(2,1)} async-done(((bf16[256,512]{1,0:T(8,128)(2,1)}), bf16[2048,512]{1,0:T(8,128)(2,1)}) %all-gather.23.cloned.1.call-update) | async-done | bytes 2097168 | tf_op jit(solution)/shard_map/all_gather | solution.py:133
  274.1 3.7 collective-permute-start
  280.2 42.6 %all-gather.17.cloned.1.call-done = bf16[512,2048]{1,0:T(8,128)(2,1)} async-done(((bf16[512,256]{1,0:T(8,128)(2,1)}), bf16[512,2048]{1,0:T(8,128)(2,1)}) %all-gather.17.cloned.1.call-update) | async-done | bytes 2097168 | tf_op jit(solution)/shard_map/all_gather | solution.py:134
  322.8 3.0 fusion.87
  327.1 45.1 %all-gather.19.cloned.1.call-done = bf16[2048,512]{1,0:T(8,128)(2,1)} async-done(((bf16[256,512]{1,0:T(8,128)(2,1)}), bf16[2048,512]{1,0:T(8,128)(2,1)}) %all-gather.19.cloned.1.call-update) | async-done | bytes 2097168 | tf_op jit(solution)/shard_map/all_gather | solution.py:131
  372.2 51.0 %all-gather.25.cloned.1.call-done = bf16[512,2048]{1,0:T(8,128)(2,1)} async-done(((bf16[512,256]{1,0:T(8,128)(2,1)}), bf16[512,2048]{1,0:T(8,128)(2,1)}) %all-gather.25.cloned.1.call-update) | async-done | bytes 2097168 | tf_op jit(solution)/shard_map/all_gather | solution.py:135
  423.2 4.4 fusion
  432.5 3.6 fusion.1
  436.2 8.8 %reduce-scatter.5.cloned.1.call-done = bf16[64,2048]{1,0:T(8,128)(2,1)} async-done(((bf16[128,2048]{1,0:T(8,128)(2,1)}), bf16[64,2048]{1,0:T(8,128)(2,1)}) %reduce-scatter.5.cloned.1.call-update) | async-done | bytes 262160 | tf_op jit(solution)/shard_map/reduce_scatter | solution.py:162
  (117 shorter events, 35.7 us)
Async XLA Ops:
  6.5 5.5 %copy-start.12 = (bf16[2,64,2048]{2,1,0:T(8,128)(2,1)S(1)}, bf16[2,64,2048]{2,1,0:T(8,128)(2,1)}, u32[]{:S(2)}) copy-start(bf16[2,64,2048]{2,1,0:T(8,128)(2,1)} %param.15) | copy-start | bytes 1572868
  6.5 54.8 %all-gather.13.cloned.1.call-start = ((), (), s32[]{:S(2)}) async-start(), calls=%async_computation.3 | async-start | bytes 2359296 | tf_op jit(solution)/shard_map/all_gather | solution.py:129
  7.3 109.6 %all-gather.11.cloned.1.call-start = ((), (), s32[]{:S(2)}) async-start(), calls=%async_computation.2 | async-start | bytes 2359296 | tf_op jit(solution)/shard_map/all_gather | solution.py:128
  8.0 162.0 %all-gather.15.cloned.1.call-start = ((), (), s32[]{:S(2)}) async-start(), calls=%async_computation.4 | async-start | bytes 2359296 | tf_op jit(solution)/shard_map/all_gather | solution.py:130
  8.7 213.2 %all-gather.21.cloned.1.call-start = ((), (), s32[]{:S(2)}) async-start(), calls=%async_computation.7 | async-start | bytes 2359296 | tf_op jit(solution)/shard_map/all_gather | solution.py:132
  9.3 262.7 %all-gather.23.cloned.1.call-start = ((), (), s32[]{:S(2)}) async-start(), calls=%async_computation.8 | async-start | bytes 2359296 | tf_op jit(solution)/shard_map/all_gather | solution.py:133
  9.9 312.9 %all-gather.17.cloned.1.call-start = ((), (), s32[]{:S(2)}) async-start(), calls=%async_computation.5 | async-start | bytes 2359296 | tf_op jit(solution)/shard_map/all_gather | solution.py:134
  10.5 6.6 %copy-start.17 = (f32[512]{0:T(512)S(1)}, f32[512]{0:T(512)}, u32[]{:S(2)}) copy-start(f32[512]{0:T(512)} %param.20) | copy-start | bytes 6148
  10.5 6.7 %copy-start.14 = (f32[3,512]{1,0:T(4,128)S(1)}, f32[3,512]{1,0:T(4,128)}, u32[]{:S(2)}) copy-start(f32[3,512]{1,0:T(4,128)} %param.27) | copy-start | bytes 18436
  10.5 50.9 %copy-start.7 = (f32[2048]{0:T(1024)S(1)}, f32[2048]{0:T(1024)}, u32[]{:S(2)}) copy-start(f32[2048]{0:T(1024)} %param.16) | copy-start | bytes 24580
  10.5 361.7 %all-gather.19.cloned.1.call-start = ((), (), s32[]{:S(2)}) async-start(), calls=%async_computation.6 | async-start | bytes 2359296 | tf_op jit(solution)/shard_map/all_gather | solution.py:131
  11.3 411.9 %all-gather.25.cloned.1.call-start = ((), (), s32[]{:S(2)}) async-start(), calls=%async_computation.9 | async-start | bytes 2359296 | tf_op jit(solution)/shard_map/all_gather | solution.py:135
  12.0 424.2 %reduce-scatter.3.cloned.1.call-start = ((), (), s32[]{:S(2)}) async-start(), calls=%async_computation.10 | async-start | bytes 786432 | tf_op jit(solution)/shard_map/reduce_scatter | solution.py:162
  61.4 6.0 %copy-start.4 = (bf16[2048,512]{1,0:T(8,128)(2,1)S(1)}, bf16[2048,512]{1,0:T(8,128)(2,1)}, u32[]{:S(2)}) copy-start(bf16[2048,512]{1,0:T(8,128)(2,1)} %all-gather.13.cloned.1.call-done) | copy-start | bytes 6291460
  119.1 26.1 %copy-start.2 = (bf16[2048,512]{1,0:T(8,128)(2,1)S(1)}, bf16[2048,512]{1,0:T(8,128)(2,1)}, u32[]{:S(2)}) copy-start(bf16[2048,512]{1,0:T(8,128)(2,1)} %all-gather.11.cloned.1.call-done) | copy-start | bytes 6291460
  274.1 5.1 %copy-start.8 = (bf16[128,512]{1,0:T(8,128)(2,1)}, bf16[128,512]{1,0:T(8,128)(2,1)S(1)}, u32[]{:S(2)}) copy-start(bf16[128,512]{1,0:T(8,128)(2,1)S(1)} %fusion.21) | copy-start | bytes 393220
  274.1 4.2 copy-start.6
  274.1 4.2 copy-start.13
  274.1 52.9 %collective-permute-start = (bf16[2,512]{1,0:T(2,128)(2,1)S(1)}, bf16[2,512]{1,0:T(2,128)(2,1)S(1)}, u32[]{:S(2)}, u32[]{:S(2)}) collective-permute-start(bf16[2,512]{1,0:T(2,128)(2,1)S(1)} %slice.73), channel_id=1, source_target_pairs={{0,4},{4,8},{8,12},{1,5},{5,9},{9,13},{2,6},{6,10},{10,14},{3,7},{... | collective-permute-start | bytes 6152 | tf_op jit(solution)/shard_map/ppermute | solution.py:21
  279.3 46.5 %copy-start.1 = (bf16[2048,512]{1,0:T(8,128)(2,1)S(1)}, bf16[2048,512]{1,0:T(8,128)(2,1)}, u32[]{:S(2)}) copy-start(bf16[2048,512]{1,0:T(8,128)(2,1)} %all-gather.21.cloned.1.call-done) | copy-start | bytes 6291460
  423.2 4.5 copy-start
  427.6 3.4 copy-start.10
  427.6 17.4 %reduce-scatter.5.cloned.1.call-start = ((), (), s32[]{:S(2)}) async-start(), calls=%async_computation.11 | async-start | bytes 786432 | tf_op jit(solution)/shard_map/reduce_scatter | solution.py:162
  429.3 3.2 collective-permute-start.1
  (7 other events, 15.5 us)
Sparse Core Ops, SparseCore 0:
  9.5 51.8 all-gather.12
  63.5 53.3 all-gather.10
  119.0 50.9 all-gather.14
  172.0 49.9 all-gather.20
  223.9 48.0 all-gather.22
  273.9 48.8 all-gather.16
  324.9 47.2 all-gather.18
  374.3 48.8 all-gather.24
  427.7 6.1 reduce-scatter.2
  436.3 8.6 reduce-scatter.4
where the time goes:
time: 454 us
  waiting for transfers between devices  298 us (66%)
  blocking collectives  82.9 us (18%)
  matrix products  37.9 us (8%)
  between operations  14 us (3%)
  local copies, waits for them, and re-layouts  8.85 us (2%)
  other arithmetic  6.18 us (1%)
  starting transfers between devices  5.72 us (1%)
    all_gather x1, waiting for transfers between devices, on_device(): lax.all_gather(w_out_conv, ('sp', 'fs'), axis=1, tiled=True)  51 us
    all_gather x1, waiting for transfers between devices, on_device(): lax.all_gather(w_conv_in, ('sp', 'fs'), axis=0, tiled=True)  48 us
    all_gather x1, waiting for transfers between devices, on_device(): lax.all_gather(w_gate_b, ('sp', 'fs'), axis=0, tiled=True)  45.1 us
    all_gather x1, waiting for transfers between devices, on_device(): lax.all_gather(w_key, ('sp', 'fs'), axis=0, tiled=True)  44.2 us
    all_gather x1, waiting for transfers between devices, on_device(): lax.all_gather(w_out_attn, ('sp', 'fs'), axis=1, tiled=True)  42.6 us
    all_gather x2, blocking collectives, attend_heads(): lax.all_gather(key.reshape(rows, heads_here * 2 * DK), 'sp', axis=0, tile...  40.8 us
    all_gather x2, blocking collectives, attend_heads(): value_piece = lax.all_gather(value, 'sp', axis=0, tiled=True)  37.6 us
    all_gather x1, waiting for transfers between devices, on_device(): lax.all_gather(w_query, ('sp', 'fs'), axis=0, tiled=True)  24.1 us
  transfers between devices with their start and end apart: 12, of which 9 were waited for; matrix products, arithmetic and copies ran while one was open for 10% of the time, Pallas kernels for 0%

commit v1 on v0

--- a/solution.py
+++ b/solution.py
@@ -3,6 +3,8 @@
 import jax
 import jax.numpy as jnp
 from jax import lax
+from jax.experimental import pallas as pl
+from jax.experimental.pallas import tpu as pltpu
 from jax.sharding import PartitionSpec as P
 
 DK = 64
@@ -172,6 +174,320 @@
     return jnp.stack(results, axis=0)
 
 
+BF16, F32 = jnp.bfloat16, jnp.float32
+ANY = pl.BlockSpec(memory_space=pl.ANY)
+VMEM = pl.BlockSpec(memory_space=pltpu.VMEM)
+SMEM = pl.BlockSpec(memory_space=pltpu.SMEM)
+SWAP = [(0, 1), (1, 0)]
+
+
+def source_of(shift, levels):
+    return lax.rem(lax.axis_index("sp") + (levels - shift), levels)
+
+
+def mixer_kernel(
+    levels, steps, seqs, half, *refs
+):
+    n_x = 2 * levels
+    n_w = 8
+    x_refs = refs[:n_x]
+    w_refs = refs[n_x : n_x + n_w]
+    norm_gain, qg, kg, lam, hg, taps = refs[n_x + n_w : n_x + n_w + 6]
+    z_ref = refs[n_x + n_w + 6]
+    x_scr, w_scr, n_scr, p_scr, x_sem, w_sem = refs[n_x + n_w + 7 :]
+    s = lax.axis_index("sp")
+    g = lax.axis_index("grp")
+    f = lax.axis_index("fs")
+    t = lax.axis_index("tp")
+    rows = 2 * half
+    length = levels * rows
+    n_f = steps
+    depth = w_refs[0].shape[2]
+    width = w_refs[0].shape[3]
+
+    x_copies = []
+    for k in range(levels):
+        src = source_of(k, levels)
+        group = []
+        for o in range(2):
+            side = t if o == 0 else 1 - t
+            for b in range(seqs):
+                at = pl.multiple_of(src * (seqs * rows) + b * rows + side * half, half)
+                c = pltpu.make_async_copy(
+                    x_refs[o * levels + k].at[b],
+                    x_scr.at[pl.ds(at, half), :],
+                    x_sem.at[k, o, b],
+                )
+                c.start()
+                group.append(c)
+        x_copies.append(group)
+    w_copies = []
+    for i in range(n_w):
+        ty = g if i < 4 else 1 - g
+        fs = f if i % 4 < 2 else 1 - f
+        h = i % 2
+        for j in range(2):
+            src = source_of(2 * h + j, levels)
+            at = pl.multiple_of((src * n_f + fs) * depth, depth)
+            for w in range(3):
+                c = pltpu.make_async_copy(
+                    w_refs[i].at[j, w],
+                    w_scr.at[ty, pl.ds(at, depth), pl.ds(w * width, width)],
+                    w_sem.at[i, j, w],
+                )
+                c.start()
+                w_copies.append(c)
+    gain = norm_gain[...]
+    step = 16
+    for k in range(levels):
+        for c in x_copies[k]:
+            c.wait()
+        base = source_of(k, levels) * (seqs * rows)
+
+        @pl.loop(0, seqs * rows // step, unroll=2)
+        def _(n):
+            at = pl.multiple_of(base + n * step, step)
+            wide = x_scr[pl.ds(at, step), :].astype(F32)
+            scale = lax.rsqrt(jnp.mean(wide * wide, axis=-1, keepdims=True) + EPS)
+            n_scr[pl.ds(at, step), :] = (wide * scale * gain).astype(BF16)
+
+    for c in w_copies:
+        c.wait()
+    lane = lax.broadcasted_iota(jnp.int32, (1, 2 * DK), 1)
+    first = lane < DK
+
+    def pair_norm(raw, own_gain):
+        wide = raw.astype(BF16).astype(F32)
+        sq = wide * wide
+        m0 = jnp.sum(jnp.where(first, sq, 0.0), axis=-1, keepdims=True) * (1.0 / DK)
+        m1 = jnp.sum(jnp.where(first, 0.0, sq), axis=-1, keepdims=True) * (1.0 / DK)
+        return wide * jnp.where(first, lax.rsqrt(m0 + EPS), lax.rsqrt(m1 + EPS)) * own_gain
+
+    q_gain = qg[pl.ds(s, 1), :]
+    k_gain = kg[pl.ds(s, 1), :]
+    for level in range(levels):
+        at = level * seqs * rows
+        normed = n_scr[at : at + seqs * rows, :]
+        for ty in range(2):
+            got = jnp.dot(normed, w_scr[ty], preferred_element_type=F32)
+            parts = [got[:, w * width : (w + 1) * width] for w in range(3)]
+            if ty == 0:
+                parts[0] = pair_norm(parts[0], q_gain) * DK ** (-0.5)
+                parts[1] = pair_norm(parts[1], k_gain)
+            for w in range(3):
+                done = parts[w].astype(BF16)
+                for b in range(seqs):
+                    p_scr[3 * ty + w, b, level * rows : (level + 1) * rows, :] = done[
+                        b * rows : (b + 1) * rows
+                    ]
+    lam_own = lam[s]
+    head_gain = hg[...]
+    row = lax.broadcasted_iota(jnp.int32, (rows, rows), 0)
+    col = lax.broadcasted_iota(jnp.int32, (rows, rows), 1)
+    seen = col <= row
+    seen = jnp.concatenate([seen, seen], axis=0)
+    for b in range(seqs):
+        shaped = (p_scr[4, b].astype(F32) * p_scr[5, b].astype(F32)).astype(BF16).astype(F32)
+        where = lax.broadcasted_iota(jnp.int32, (length, 1), 0)
+        conv = taps[KW - 1, pl.ds(s, 1), :] * shaped
+        for back in range(1, KW):
+            moved = jnp.where(where >= back, pltpu.roll(shaped, back, 0), 0.0)
+            conv = conv + taps[KW - 1 - back, pl.ds(s, 1), :] * moved
+        conv_out = (p_scr[3, b].astype(F32) * conv).astype(BF16)
+        for i in range(levels):
+            to = lax.rem(i - s + levels, levels)
+            z_ref[to, b, :, width:] = conv_out[i * rows : (i + 1) * rows]
+            q = p_scr[0, b, i * rows : (i + 1) * rows, :]
+            zero = jnp.zeros_like(q)
+            q2 = jnp.concatenate([jnp.where(first, q, zero), jnp.where(first, zero, q)], axis=0)
+            upto = (i + 1) * rows
+            score = lax.dot_general(
+                q2,
+                p_scr[1, b, :upto, :],
+                (((1,), (1,)), ((), ())),
+                preferred_element_type=F32,
+            )
+            edge = jnp.where(seen, score[:, i * rows :], NEG)
+            if i > 0:
+                score = jnp.concatenate([score[:, : i * rows], edge], axis=1)
+            else:
+                score = edge
+            top = jnp.max(score, axis=-1, keepdims=True)
+            weights = jnp.exp(score - top)
+            total = jnp.sum(weights, axis=-1, keepdims=True)
+            summed = jnp.dot(
+                weights.astype(BF16), p_scr[2, b, :upto, :], preferred_element_type=F32
+            )
+            maps = summed / total
+            differ = maps[:rows] - lam_own * maps[rows:]
+            scale = lax.rsqrt(jnp.mean(differ * differ, axis=-1, keepdims=True) + EPS)
+            z_ref[to, b, :, :width] = (differ * scale * head_gain * OUT_SCALE).astype(BF16)
+
+
+def output_kernel(levels, steps, seqs, half, *refs):
+    z_refs = refs[:levels]
+    w_refs = refs[levels : levels + 8]
+    keep_ref, send_ref = refs[levels + 8 : levels + 10]
+    z_scr, w_scr, w_sem = refs[levels + 10 :]
+    g = lax.axis_index("grp")
+    f = lax.axis_index("fs")
+    t = lax.axis_index("tp")
+    rows = 2 * half
+    width = z_refs[0].shape[2] // 2
+    columns = w_refs[0].shape[2]
+    copies = []
+    for i in range(8):
+        ty = g if i < 4 else 1 - g
+        pair = []
+        for j in range(2):
+            c = pltpu.make_async_copy(w_refs[i].at[j], w_scr.at[ty, i % 4, j], w_sem.at[i, j])
+            c.start()
+            pair.append(c)
+        copies.append(pair)
+    for k in range(levels):
+        at = pl.multiple_of(source_of(k, levels) * width, width)
+        for b in range(seqs):
+            for ty in range(2):
+                z_scr[ty, b * rows : (b + 1) * rows, pl.ds(at, width)] = z_refs[k][
+                    b, :, ty * width : (ty + 1) * width
+                ]
+    for q in range(4):
+        fs = f if q < 2 else 1 - f
+        for j in range(2):
+            copies[q][j].wait()
+            copies[q + 4][j].wait()
+            got = jnp.dot(z_scr[0], w_scr[0, q, j], preferred_element_type=F32) + jnp.dot(
+                z_scr[1], w_scr[1, q, j], preferred_element_type=F32
+            )
+            src = source_of(2 * (q % 2) + j, levels)
+            at = pl.multiple_of((src * steps + fs) * columns, columns)
+            for b in range(seqs):
+                low = got[b * rows : b * rows + half]
+                high = got[b * rows + half : (b + 1) * rows]
+                keep_ref[b, :, pl.ds(at, columns)] = jnp.where(t == 0, low, high)
+                send_ref[b, :, pl.ds(at, columns)] = jnp.where(t == 0, high, low).astype(BF16)
+
+
+def both_ways(halves):
+    first, second = halves
+    first_x = lax.ppermute(first, "fs", SWAP)
+    second_y = lax.ppermute(second, "grp", SWAP)
+    first_y = lax.ppermute(first, "grp", SWAP)
+    second_x = lax.ppermute(second, "fs", SWAP)
+    first_xy = lax.ppermute(first_x, "grp", SWAP)
+    second_xy = lax.ppermute(second_y, "fs", SWAP)
+    return [first, second, first_x, second_x, first_y, second_y, first_xy, second_xy]
+
+
+def relayed_device(
+    tokens,
+    norm_gain,
+    w_query,
+    w_key,
+    w_value,
+    query_gain,
+    key_gain,
+    mix_lambda,
+    head_gain,
+    w_gate_b,
+    w_gate_c,
+    w_conv_in,
+    conv_taps,
+    w_out_attn,
+    w_out_conv,
+):
+    levels = lax.axis_size("sp")
+    steps = lax.axis_size("fs")
+    s = lax.axis_index("sp")
+    g = lax.axis_index("grp")
+    seqs, half, model = tokens.shape
+    depth, wide = w_query.shape
+    width = wide // levels
+    up = [(i, i + 1) for i in range(levels - 1)]
+    down = [(i + 1, i) for i in range(levels - 1)]
+
+    def shifted(block, k):
+        return lax.ppermute(block, "sp", [(i, (i + k) % levels) for i in range(levels)])
+
+    from_below = [tokens]
+    from_above = [tokens]
+    from_below.append(lax.ppermute(from_below[-1], "sp", up))
+    from_above.append(lax.ppermute(from_above[-1], "sp", down))
+
+    mine = jnp.where(
+        g == 0, jnp.stack([w_query, w_key, w_value]), jnp.stack([w_gate_b, w_gate_c, w_conv_in])
+    )
+    pieces = []
+    for k in range(levels):
+        at = lax.rem(s + k, levels) * width
+        piece = lax.dynamic_slice(mine, (0, 0, at), (3, depth, width))
+        pieces.append(shifted(piece, k) if k else piece)
+    w_parts = both_ways([jnp.stack(pieces[:2]), jnp.stack(pieces[2:])])
+
+    own_out = jnp.where(g == 0, w_out_attn, w_out_conv)
+    outs = [own_out] + [shifted(own_out, k) for k in range(1, levels)]
+    o_parts = both_ways([jnp.stack(outs[:2]), jnp.stack(outs[2:])])
+
+    for k in range(2, levels):
+        from_below.append(lax.ppermute(from_below[-1], "sp", up))
+        from_above.append(lax.ppermute(from_above[-1], "sp", down))
+    blocks = [tokens] + [
+        jnp.where(s >= k, from_below[k], from_above[levels - k]) for k in range(1, levels)
+    ]
+    others = [lax.ppermute(block, "tp", SWAP) for block in blocks]
+
+    z = pl.pallas_call(
+        lambda *refs: mixer_kernel(levels, steps, seqs, half, *refs),
+        out_shape=jax.ShapeDtypeStruct((levels, seqs, 2 * half, 2 * width), BF16),
+        in_specs=[ANY] * (2 * levels + 8) + [VMEM, VMEM, VMEM, SMEM, VMEM, VMEM],
+        out_specs=VMEM,
+        scratch_shapes=[
+            pltpu.VMEM((levels * seqs * 2 * half, model), BF16),
+            pltpu.VMEM((2, model, 3 * width), BF16),
+            pltpu.VMEM((levels * seqs * 2 * half, model), BF16),
+            pltpu.VMEM((6, seqs, levels * 2 * half, width), BF16),
+            pltpu.SemaphoreType.DMA((levels, 2, seqs)),
+            pltpu.SemaphoreType.DMA((8, 2, 3)),
+        ],
+        compiler_params=pltpu.CompilerParams(vmem_limit_bytes=48 * 1024 * 1024),
+        cost_estimate=pl.CostEstimate(
+            flops=8_000_000_000, bytes_accessed=8_000_000, transcendentals=1_000_000
+        ),
+        name="mixer",
+    )(
+        *blocks,
+        *others,
+        *w_parts,
+        norm_gain.reshape(1, model),
+        query_gain.reshape(levels, 2 * DK),
+        key_gain.reshape(levels, 2 * DK),
+        mix_lambda,
+        head_gain.reshape(1, DV),
+        conv_taps.reshape(KW, levels, width),
+    )
+    arrived = [z[0]] + [shifted(z[k], k) for k in range(1, levels)]
+    keep, send = pl.pallas_call(
+        lambda *refs: output_kernel(levels, steps, seqs, half, *refs),
+        out_shape=(
+            jax.ShapeDtypeStruct((seqs, half, model), F32),
+            jax.ShapeDtypeStruct((seqs, half, model), BF16),
+        ),
+        in_specs=[VMEM] * levels + [ANY] * 8,
+        out_specs=(VMEM, VMEM),
+        scratch_shapes=[
+            pltpu.VMEM((2, seqs * 2 * half, wide), BF16),
+            pltpu.VMEM((2, 4, 2, wide, w_out_attn.shape[1]), BF16),
+            pltpu.SemaphoreType.DMA((8, 2)),
+        ],
+        compiler_params=pltpu.CompilerParams(vmem_limit_bytes=32 * 1024 * 1024),
+        cost_estimate=pl.CostEstimate(
+            flops=2_000_000_000, bytes_accessed=8_000_000, transcendentals=0
+        ),
+        name="output",
+    )(*arrived, *o_parts)
+    return (keep + lax.ppermute(send, "tp", SWAP).astype(F32)).astype(BF16)
+
+
 def solution(mesh):
     placed = (
         P(("grp", "fs"), ("sp", "tp"), None),
@@ -190,10 +506,23 @@
         P("tp", ("sp", "fs")),
         P("tp", ("sp", "fs")),
     )
-    return jax.shard_map(
-        on_device,
+    grid = mesh.shape
+    relayed = grid["grp"] == 2 and grid["fs"] == 2 and grid["tp"] == 2 and grid["sp"] == 4
+
+    def layer(*arrays):
+        alike = arrays[2].shape == arrays[4].shape == arrays[9].shape
+        one_head = arrays[7].shape[0] == grid["sp"] * grid["tp"]
+        if relayed and alike and one_head:
+            body = relayed_device
+        else:
+            body = on_device
+        return sharded(body)(*arrays)
+
+    sharded = lambda body: jax.shard_map(
+        body,
         mesh=mesh,
         in_specs=placed,
         out_specs=P(("grp", "fs"), ("sp", "tp"), None),
         check_vma=False,
     )
+    return layer

time: 454 us -> 155 us (0.34)
  waiting for transfers between devices: 298 us -> 65.1 us
  blocking collectives: 82.9 us -> 0 us
  starting transfers between devices: 5.72 us -> 59.3 us
  matrix products: 37.9 us -> 0 us
  Pallas kernels: 0 us -> 17.4 us
  between operations: 14 us -> 0.35 us
    all_gather x8 -> x0, waiting for transfers between devices: 284 us -> none  [the longest x1 51 us: on_device(): lax.all_gather(w_out_conv, ('sp', 'fs'), axis=1, tiled=True)]
    all_gather x6 -> x0, blocking collectives: 82.9 us -> none  [the longest x2 40.8 us: attend_heads(): lax.all_gather(key.reshape(rows, heads_here * 2 * DK), 'sp', axis=0, tile...]
    ppermute x2 -> x32, waiting for transfers between devices: 0.01 us -> 65.1 us  [the longest x9 28.4 us: shifted(): lax.ppermute(block, 'sp', [(i, (i + k) % levels) for i in range(levels)])]
    ppermute x2 -> x32, starting transfers between devices: 5.37 us -> 59.3 us  [the longest x3 26 us: relayed_device(): from_below.append(lax.ppermute(from_below[-1], 'sp', up))]
    dot_general x18 -> x0, matrix products: 37.9 us -> none  [the longest x2 8.02 us: on_device(): jnp.dot(conv_out, out_conv, preferred_element_type=jnp.float32)]
    pallas_call x0 -> x2, Pallas kernels: none -> 17.4 us  [the longest x1 13.4 us: relayed_device(): pl.pallas_call(lambda *refs: mixer_kernel(levels, steps, seqs, half, *ref...]
    reduce_scatter x2 -> x0, waiting for transfers between devices: 8.86 us -> none  [on_device(): lax.psum_scatter((jnp.dot(attn, out_attn, preferred_element_type=jnp.floa...]
    unnamed x38 -> x44, local copies, waits for them, and re-layouts: 0.09 us -> 6.8 us
  transfers between devices with their start and end apart: 12 -> 32, of which waited for: 9 -> 10; matrix products, arithmetic and copies ran while one was open for 10% -> 3% of each run, Pallas kernels for 0% -> 9%
where the time goes in v1:
time: 155 us
  waiting for transfers between devices  65.1 us (42%)
  starting transfers between devices  59.3 us (38%)
  Pallas kernels  17.4 us (11%)
  local copies, waits for them, and re-layouts  7 us (5%)
  other arithmetic  5.74 us (4%)
    ppermute x9, waiting for transfers between devices, shifted(): lax.ppermute(block, 'sp', [(i, (i + k) % levels) for i in range(levels)])  28.4 us
    ppermute x3, starting transfers between devices, relayed_device(): from_below.append(lax.ppermute(from_below[-1], 'sp', up))  26 us
    ppermute x9, starting transfers between devices, shifted(): lax.ppermute(block, 'sp', [(i, (i + k) % levels) for i in range(levels)])  15.3 us
    pallas_call x1, Pallas kernels, relayed_device(): pl.pallas_call(lambda *refs: mixer_kernel(levels, steps, seqs, half, *ref...  13.4 us
    ppermute x3, waiting for transfers between devices, relayed_device(): from_above.append(lax.ppermute(from_above[-1], 'sp', down))  13.2 us
    ppermute x2, waiting for transfers between devices, both_ways(): first_x = lax.ppermute(first, 'fs', SWAP)  7.79 us
    unnamed x44, local copies, waits for them, and re-layouts  6.8 us
    ppermute x2, waiting for transfers between devices, both_ways(): second_xy = lax.ppermute(second_y, 'fs', SWAP)  6.67 us
  transfers between devices with their start and end apart: 32, of which 10 were waited for; matrix products, arithmetic and copies ran while one was open for 3% of the time, Pallas kernels for 9%

profile of v1, /device:TPU:0, one launch (start us, length us, event | category | flops | bytes accessed | tf_op | source)
XLA Modules:
  0.0 154.8 jit_solution(9606937775851485319)
XLA Ops:
  1.3 5.6 %collective-permute-start = (bf16[2,64,2048]{2,1,0:T(8,128)(2,1)}, bf16[2,64,2048]{2,1,0:T(8,128)(2,1)S(1)}, u32[]{:S(2)}, u32[]{:S(2)}) collective-permute-start(bf16[2,64,2048]{2,1,0:T(8,128)(2,1)} %refs_0_.1), channel_id=1, source_target_pairs={{0,4},{4,8},{8,12},{1,5},{5,9},{9,13},{2,6},{6,10},{10,14},{3,7},{... | collective-permute-start | bytes 1572872 | tf_op jit(solution)/shard_map/ppermute | solution.py:414
  7.0 1.5 maximum_select_fusion
  8.6 3.1 %collective-permute-start.11 = (bf16[3,256,128]{2,1,0:T(8,128)(2,1)S(1)}, bf16[3,256,128]{2,1,0:T(8,128)(2,1)}, u32[]{:S(2)}, u32[]{:S(2)}) collective-permute-start(bf16[3,256,128]{2,1,0:T(8,128)(2,1)S(1)} %get-tuple-element.9), channel_id=1, source_target_pairs={{0,8},{4,12},{8,0},{12,4},{1,9},{5,13},{9,1},{13,5},{2,10},{6,14},... | collective-permute-start | bytes 589832 | tf_op jit(solution)/shard_map/ppermute | solution.py:410
  13.8 4.8 %collective-permute-done.1 = bf16[2,64,2048]{2,1,0:T(8,128)(2,1)S(1)} collective-permute-done((bf16[2,64,2048]{2,1,0:T(8,128)(2,1)}, bf16[2,64,2048]{2,1,0:T(8,128)(2,1)S(1)}, u32[]{:S(2)}, u32[]{:S(2)}) %collective-permute-start.1) | collective-permute-done | bytes 524320 | tf_op jit(solution)/shard_map/ppermute | solution.py:415
  19.8 12.7 %collective-permute-start.4 = (bf16[2,64,2048]{2,1,0:T(8,128)(2,1)S(1)}, bf16[2,64,2048]{2,1,0:T(8,128)(2,1)}, u32[]{:S(2)}, u32[]{:S(2)}) collective-permute-start(bf16[2,64,2048]{2,1,0:T(8,128)(2,1)S(1)} %collective-permute-done), channel_id=1, source_target_pairs={{0,4},{4,8},{8,12},{1,5},{5,9},{9,13},{2,6},{6,10},{10,14},{3,7},{... | collective-permute-start | bytes 1572872 | tf_op jit(solution)/shard_map/ppermute | solution.py:432
  34.5 3.2 %collective-permute-start.24 = (bf16[512,256]{1,0:T(8,128)(2,1)S(1)}, bf16[512,256]{1,0:T(8,128)(2,1)}, u32[]{:S(2)}, u32[]{:S(2)}) collective-permute-start(bf16[512,256]{1,0:T(8,128)(2,1)S(1)} %broadcast_select_fusion.3), channel_id=1, source_target_pairs={{0,12},{4,0},{8,4},{12,8},{1,13},{5,1},{9,5},{13,9},{2,14},{6,2},{... | collective-permute-start | bytes 786440 | tf_op jit(solution)/shard_map/ppermute | solution.py:410
  40.4 23.9 %collective-permute-done.23 = bf16[512,256]{1,0:T(8,128)(2,1)S(1)} collective-permute-done((bf16[512,256]{1,0:T(8,128)(2,1)S(1)}, bf16[512,256]{1,0:T(8,128)(2,1)S(1)}, u32[]{:S(2)}, u32[]{:S(2)}) %collective-permute-start.23) | collective-permute-done | bytes 262176 | tf_op jit(solution)/shard_map/ppermute | solution.py:410
  64.3 1.6 %collective-permute-start.16 = (bf16[2,3,256,128]{3,2,1,0:T(8,128)(2,1)S(1)}, bf16[2,3,256,128]{3,2,1,0:T(8,128)(2,1)}, u32[]{:S(2)}, u32[]{:S(2)}) collective-permute-start(bf16[2,3,256,128]{3,2,1,0:T(8,128)(2,1)S(1)} %pad_maximum_fusion.3.refs_9_), channel_id=1, source_target_pairs={{0,16},{16,0},{1,17},{17,1},{2,18},{18,2},{3,19},{19,3},{4,20},{20... | collective-permute-start | bytes 1179656 | tf_op jit(solution)/shard_map/ppermute | solution.py:374
  66.9 1.6 %collective-permute-start.14 = (bf16[2,3,256,128]{3,2,1,0:T(8,128)(2,1)S(1)}, bf16[2,3,256,128]{3,2,1,0:T(8,128)(2,1)S(1)}, u32[]{:S(2)}, u32[]{:S(2)}) collective-permute-start(bf16[2,3,256,128]{3,2,1,0:T(8,128)(2,1)S(1)} %pad_maximum_fusion.3.refs_9_), channel_id=1, source_target_pairs={{0,2},{2,0},{1,3},{3,1},{4,6},{6,4},{5,7},{7,5},{8,10},{10,8},{9,1... | collective-permute-start | bytes 1179656 | tf_op jit(solution)/shard_map/ppermute | solution.py:376
  69.8 7.6 %collective-permute-start.5 = (bf16[2,64,2048]{2,1,0:T(8,128)(2,1)}, bf16[2,64,2048]{2,1,0:T(8,128)(2,1)S(1)}, u32[]{:S(2)}, u32[]{:S(2)}) collective-permute-start(bf16[2,64,2048]{2,1,0:T(8,128)(2,1)} %collective-permute-done.4), channel_id=1, source_target_pairs={{0,4},{4,8},{8,12},{1,5},{5,9},{9,13},{2,6},{6,10},{10,14},{3,7},{... | collective-permute-start | bytes 1572872 | tf_op jit(solution)/shard_map/ppermute | solution.py:432
  77.6 8.4 %collective-permute-done.3 = bf16[2,64,2048]{2,1,0:T(8,128)(2,1)S(1)} collective-permute-done((bf16[2,64,2048]{2,1,0:T(8,128)(2,1)S(1)}, bf16[2,64,2048]{2,1,0:T(8,128)(2,1)S(1)}, u32[]{:S(2)}, u32[]{:S(2)}) %collective-permute-start.3) | collective-permute-done | bytes 524320 | tf_op jit(solution)/shard_map/ppermute | solution.py:433
  87.2 1.5 collective-permute-start.28
  90.3 7.8 %collective-permute-done.13.refs_10_ = bf16[2,3,256,128]{3,2,1,0:T(8,128)(2,1)} collective-permute-done((bf16[2,3,256,128]{3,2,1,0:T(8,128)(2,1)S(1)}, bf16[2,3,256,128]{3,2,1,0:T(8,128)(2,1)}, u32[]{:S(2)}, u32[]{:S(2)}) %collective-permute-start.13) | collective-permute-done | bytes 393248 | tf_op jit(solution)/shard_map/ppermute | solution.py:373
  100.1 6.3 %collective-permute-done.28.refs_9_ = bf16[2,512,256]{2,1,0:T(8,128)(2,1)S(1)} collective-permute-done((bf16[2,512,256]{2,1,0:T(8,128)(2,1)S(1)}, bf16[2,512,256]{2,1,0:T(8,128)(2,1)S(1)}, u32[]{:S(2)}, u32[]{:S(2)}) %collective-permute-start.28) | collective-permute-done | bytes 524320 | tf_op jit(solution)/shard_map/ppermute | solution.py:374
  109.3 6.7 %collective-permute-done.18.refs_15_ = bf16[2,3,256,128]{3,2,1,0:T(8,128)(2,1)} collective-permute-done((bf16[2,3,256,128]{3,2,1,0:T(8,128)(2,1)}, bf16[2,3,256,128]{3,2,1,0:T(8,128)(2,1)}, u32[]{:S(2)}, u32[]{:S(2)}) %collective-permute-start.18) | collective-permute-done | bytes 393248 | tf_op jit(solution)/shard_map/ppermute | solution.py:378
  116.0 1.8 %collective-permute-start.26 = (bf16[2,512,256]{2,1,0:T(8,128)(2,1)S(1)}, bf16[2,512,256]{2,1,0:T(8,128)(2,1)S(1)}, u32[]{:S(2)}, u32[]{:S(2)}) collective-permute-start(bf16[2,512,256]{2,1,0:T(8,128)(2,1)S(1)} %pad_maximum_fusion.1.refs_5_), channel_id=1, source_target_pairs={{0,2},{2,0},{1,3},{3,1},{4,6},{6,4},{5,7},{7,5},{8,10},{10,8},{9,1... | collective-permute-start | bytes 1572872 | tf_op jit(solution)/shard_map/ppermute | solution.py:376
  119.6 1.5 collective-permute-start.29
  124.9 13.4 %mixer.1 = bf16[4,2,128,256]{3,2,1,0:T(8,128)(2,1)S(1)} custom-call(bf16[2,64,2048]{2,1,0:T(8,128)(2,1)S(1)} %copy-done.1, bf16[2,64,2048]{2,1,0:T(8,128)(2,1)S(1)} %broadcast_select_fusion.2.refs_1_, bf16[2,64,2048]{2,1,0:T(8,128)(2,1)S(1)} %broadcast_select_fusion.1.refs_2_, bf16[2,64,2048]{2,1,0:T(8,128)(2,1)S(1)} %broadcast_select_fusion.refs_3_, ...), custom_call_target="tpu_custom_call" | custom-call | flops 8000000000 | bytes 8000000 | tf_op jit(solution)/shard_map/mixer/pallas_call | solution.py:439
  138.3 1.8 %collective-permute-start.19 = (bf16[2,128,256]{2,1,0:T(8,128)(2,1)S(1)}, bf16[2,128,256]{2,1,0:T(8,128)(2,1)S(1)}, u32[]{:S(2)}, u32[]{:S(2)}) collective-permute-start(bf16[2,128,256]{2,1,0:T(8,128)(2,1)S(1)} %get-tuple-element.15), channel_id=1, source_target_pairs={{0,4},{4,8},{8,12},{12,0},{1,5},{5,9},{9,13},{13,1},{2,6},{6,10},{... | collective-permute-start | bytes 393224 | tf_op jit(solution)/shard_map/ppermute | solution.py:410
  140.7 2.8 %collective-permute-start.21 = (bf16[2,128,256]{2,1,0:T(8,128)(2,1)S(1)}, bf16[2,128,256]{2,1,0:T(8,128)(2,1)S(1)}, u32[]{:S(2)}, u32[]{:S(2)}) collective-permute-start(bf16[2,128,256]{2,1,0:T(8,128)(2,1)S(1)} %get-tuple-element.13), channel_id=1, source_target_pairs={{0,12},{4,0},{8,4},{12,8},{1,13},{5,1},{9,5},{13,9},{2,14},{6,2},{... | collective-permute-start | bytes 393224 | tf_op jit(solution)/shard_map/ppermute | solution.py:410
  143.5 1.8 %collective-permute-done.19.refs_1_ = bf16[2,128,256]{2,1,0:T(8,128)(2,1)S(1)} collective-permute-done((bf16[2,128,256]{2,1,0:T(8,128)(2,1)S(1)}, bf16[2,128,256]{2,1,0:T(8,128)(2,1)S(1)}, u32[]{:S(2)}, u32[]{:S(2)}) %collective-permute-start.19) | collective-permute-done | bytes 131104 | tf_op jit(solution)/shard_map/ppermute | solution.py:410
  145.3 2.7 %collective-permute-done.20.refs_2_ = bf16[2,128,256]{2,1,0:T(8,128)(2,1)S(1)} collective-permute-done((bf16[2,128,256]{2,1,0:T(8,128)(2,1)S(1)}, bf16[2,128,256]{2,1,0:T(8,128)(2,1)S(1)}, u32[]{:S(2)}, u32[]{:S(2)}) %collective-permute-start.20) | collective-permute-done | bytes 131104 | tf_op jit(solution)/shard_map/ppermute | solution.py:410
  148.0 4.0 %output.1 = (f32[2,64,2048]{2,1,0:T(8,128)S(1)}, bf16[2,64,2048]{2,1,0:T(8,128)(2,1)S(1)}) custom-call(bf16[2,128,256]{2,1,0:T(8,128)(2,1)S(1)} %get-tuple-element.16.refs_0_, bf16[2,128,256]{2,1,0:T(8,128)(2,1)S(1)} %collective-permute-done.19.refs_1_, bf16[2,128,256]{2,1,0:T(8,128)(2,1)S(1)} %collective-permute-done.20.refs_2_, ...), custom_call_target="tpu_custom_call" | custom-call | flops 2000000000 | bytes 8000000 | tf_op jit(solution)/shard_map/output/pallas_call | solution.py:469
  152.0 1.9 %collective-permute-done.31 = bf16[2,64,2048]{2,1,0:T(8,128)(2,1)S(1)} collective-permute-done((bf16[2,64,2048]{2,1,0:T(8,128)(2,1)S(1)}, bf16[2,64,2048]{2,1,0:T(8,128)(2,1)S(1)}, u32[]{:S(2)}, u32[]{:S(2)}) %collective-permute-start.31) | collective-permute-done | bytes 524320 | tf_op jit(solution)/shard_map/ppermute | solution.py:488
  (99 shorter events, 26.5 us)
Async XLA Ops:
  0.0 18.5 %collective-permute-start.1 = (bf16[2,64,2048]{2,1,0:T(8,128)(2,1)}, bf16[2,64,2048]{2,1,0:T(8,128)(2,1)S(1)}, u32[]{:S(2)}, u32[]{:S(2)}) collective-permute-start(bf16[2,64,2048]{2,1,0:T(8,128)(2,1)} %refs_0_.1), channel_id=1, source_target_pairs={{4,0},{8,4},{12,8},{5,1},{9,5},{13,9},{6,2},{10,6},{14,10},{7,3},{... | collective-permute-start | bytes 1572872 | tf_op jit(solution)/shard_map/ppermute | solution.py:415
  1.3 18.5 %collective-permute-start = (bf16[2,64,2048]{2,1,0:T(8,128)(2,1)}, bf16[2,64,2048]{2,1,0:T(8,128)(2,1)S(1)}, u32[]{:S(2)}, u32[]{:S(2)}) collective-permute-start(bf16[2,64,2048]{2,1,0:T(8,128)(2,1)} %refs_0_.1), channel_id=1, source_target_pairs={{0,4},{4,8},{8,12},{1,5},{5,9},{9,13},{2,6},{6,10},{10,14},{3,7},{... | collective-permute-start | bytes 1572872 | tf_op jit(solution)/shard_map/ppermute | solution.py:414
  8.6 23.9 %collective-permute-start.11 = (bf16[3,256,128]{2,1,0:T(8,128)(2,1)S(1)}, bf16[3,256,128]{2,1,0:T(8,128)(2,1)}, u32[]{:S(2)}, u32[]{:S(2)}) collective-permute-start(bf16[3,256,128]{2,1,0:T(8,128)(2,1)S(1)} %get-tuple-element.9), channel_id=1, source_target_pairs={{0,8},{4,12},{8,0},{12,4},{1,9},{5,13},{9,1},{13,5},{2,10},{6,14},... | collective-permute-start | bytes 589832 | tf_op jit(solution)/shard_map/ppermute | solution.py:410
  11.7 22.1 %collective-permute-start.12 = (bf16[3,256,128]{2,1,0:T(8,128)(2,1)S(1)}, bf16[3,256,128]{2,1,0:T(8,128)(2,1)S(1)}, u32[]{:S(2)}, u32[]{:S(2)}) collective-permute-start(bf16[3,256,128]{2,1,0:T(8,128)(2,1)S(1)} %get-tuple-element.10), channel_id=1, source_target_pairs={{0,12},{4,0},{8,4},{12,8},{1,13},{5,1},{9,5},{13,9},{2,14},{6,2},{... | collective-permute-start | bytes 589832 | tf_op jit(solution)/shard_map/ppermute | solution.py:410
  13.1 24.7 %collective-permute-start.10 = (bf16[3,256,128]{2,1,0:T(8,128)(2,1)S(1)}, bf16[3,256,128]{2,1,0:T(8,128)(2,1)}, u32[]{:S(2)}, u32[]{:S(2)}) collective-permute-start(bf16[3,256,128]{2,1,0:T(8,128)(2,1)S(1)} %get-tuple-element.11), channel_id=1, source_target_pairs={{0,4},{4,8},{8,12},{12,0},{1,5},{5,9},{9,13},{13,1},{2,6},{6,10},{... | collective-permute-start | bytes 589832 | tf_op jit(solution)/shard_map/ppermute | solution.py:410
  18.5 49.9 %collective-permute-start.2 = (bf16[2,64,2048]{2,1,0:T(8,128)(2,1)S(1)}, bf16[2,64,2048]{2,1,0:T(8,128)(2,1)S(1)}, u32[]{:S(2)}, u32[]{:S(2)}) collective-permute-start(bf16[2,64,2048]{2,1,0:T(8,128)(2,1)S(1)} %collective-permute-done.1), channel_id=1, source_target_pairs={{4,0},{8,4},{12,8},{5,1},{9,5},{13,9},{6,2},{10,6},{14,10},{7,3},{... | collective-permute-start | bytes 1572872 | tf_op jit(solution)/shard_map/ppermute | solution.py:433
  19.8 50.0 %collective-permute-start.4 = (bf16[2,64,2048]{2,1,0:T(8,128)(2,1)S(1)}, bf16[2,64,2048]{2,1,0:T(8,128)(2,1)}, u32[]{:S(2)}, u32[]{:S(2)}) collective-permute-start(bf16[2,64,2048]{2,1,0:T(8,128)(2,1)S(1)} %collective-permute-done), channel_id=1, source_target_pairs={{0,4},{4,8},{8,12},{1,5},{5,9},{9,13},{2,6},{6,10},{10,14},{3,7},{... | collective-permute-start | bytes 1572872 | tf_op jit(solution)/shard_map/ppermute | solution.py:432
  32.6 31.7 %collective-permute-start.23 = (bf16[512,256]{1,0:T(8,128)(2,1)S(1)}, bf16[512,256]{1,0:T(8,128)(2,1)S(1)}, u32[]{:S(2)}, u32[]{:S(2)}) collective-permute-start(bf16[512,256]{1,0:T(8,128)(2,1)S(1)} %broadcast_select_fusion.3), channel_id=1, source_target_pairs={{0,8},{4,12},{8,0},{12,4},{1,9},{5,13},{9,1},{13,5},{2,10},{6,14},... | collective-permute-start | bytes 786440 | tf_op jit(solution)/shard_map/ppermute | solution.py:410
  34.5 29.8 %collective-permute-start.24 = (bf16[512,256]{1,0:T(8,128)(2,1)S(1)}, bf16[512,256]{1,0:T(8,128)(2,1)}, u32[]{:S(2)}, u32[]{:S(2)}) collective-permute-start(bf16[512,256]{1,0:T(8,128)(2,1)S(1)} %broadcast_select_fusion.3), channel_id=1, source_target_pairs={{0,12},{4,0},{8,4},{12,8},{1,13},{5,1},{9,5},{13,9},{2,14},{6,2},{... | collective-permute-start | bytes 786440 | tf_op jit(solution)/shard_map/ppermute | solution.py:410
  37.7 29.2 %collective-permute-start.22 = (bf16[512,256]{1,0:T(8,128)(2,1)S(1)}, bf16[512,256]{1,0:T(8,128)(2,1)S(1)}, u32[]{:S(2)}, u32[]{:S(2)}) collective-permute-start(bf16[512,256]{1,0:T(8,128)(2,1)S(1)} %broadcast_select_fusion.3), channel_id=1, source_target_pairs={{0,4},{4,8},{8,12},{12,0},{1,5},{5,9},{9,13},{13,1},{2,6},{6,10},{... | collective-permute-start | bytes 786440 | tf_op jit(solution)/shard_map/ppermute | solution.py:410
  64.3 22.3 %collective-permute-start.6 = (bf16[2,64,2048]{2,1,0:T(8,128)(2,1)S(1)}, bf16[2,64,2048]{2,1,0:T(8,128)(2,1)S(1)}, u32[]{:S(2)}, u32[]{:S(2)}) collective-permute-start(bf16[2,64,2048]{2,1,0:T(8,128)(2,1)S(1)} %copy-done), channel_id=1, source_target_pairs={{0,1},{1,0},{2,3},{3,2},{4,5},{5,4},{6,7},{7,6},{8,9},{9,8},{10,11... | collective-permute-start | bytes 1572872 | tf_op jit(solution)/shard_map/ppermute | solution.py:437
  64.3 22.8 %collective-permute-start.16 = (bf16[2,3,256,128]{3,2,1,0:T(8,128)(2,1)S(1)}, bf16[2,3,256,128]{3,2,1,0:T(8,128)(2,1)}, u32[]{:S(2)}, u32[]{:S(2)}) collective-permute-start(bf16[2,3,256,128]{3,2,1,0:T(8,128)(2,1)S(1)} %pad_maximum_fusion.3.refs_9_), channel_id=1, source_target_pairs={{0,16},{16,0},{1,17},{17,1},{2,18},{18,2},{3,19},{19,3},{4,20},{20... | collective-permute-start | bytes 1179656 | tf_op jit(solution)/shard_map/ppermute | solution.py:374
  66.9 31.1 %collective-permute-start.14 = (bf16[2,3,256,128]{3,2,1,0:T(8,128)(2,1)S(1)}, bf16[2,3,256,128]{3,2,1,0:T(8,128)(2,1)S(1)}, u32[]{:S(2)}, u32[]{:S(2)}) collective-permute-start(bf16[2,3,256,128]{3,2,1,0:T(8,128)(2,1)S(1)} %pad_maximum_fusion.3.refs_9_), channel_id=1, source_target_pairs={{0,2},{2,0},{1,3},{3,1},{4,6},{6,4},{5,7},{7,5},{8,10},{10,8},{9,1... | collective-permute-start | bytes 1179656 | tf_op jit(solution)/shard_map/ppermute | solution.py:376
  68.5 17.5 %collective-permute-start.3 = (bf16[2,64,2048]{2,1,0:T(8,128)(2,1)S(1)}, bf16[2,64,2048]{2,1,0:T(8,128)(2,1)S(1)}, u32[]{:S(2)}, u32[]{:S(2)}) collective-permute-start(bf16[2,64,2048]{2,1,0:T(8,128)(2,1)S(1)} %collective-permute-done.2), channel_id=1, source_target_pairs={{4,0},{8,4},{12,8},{5,1},{9,5},{13,9},{6,2},{10,6},{14,10},{7,3},{... | collective-permute-start | bytes 1572872 | tf_op jit(solution)/shard_map/ppermute | solution.py:433
  69.8 18.8 %collective-permute-start.5 = (bf16[2,64,2048]{2,1,0:T(8,128)(2,1)}, bf16[2,64,2048]{2,1,0:T(8,128)(2,1)S(1)}, u32[]{:S(2)}, u32[]{:S(2)}) collective-permute-start(bf16[2,64,2048]{2,1,0:T(8,128)(2,1)} %collective-permute-done.4), channel_id=1, source_target_pairs={{0,4},{4,8},{8,12},{1,5},{5,9},{9,13},{2,6},{6,10},{10,14},{3,7},{... | collective-permute-start | bytes 1572872 | tf_op jit(solution)/shard_map/ppermute | solution.py:432
  87.2 19.3 %collective-permute-start.28 = (bf16[2,512,256]{2,1,0:T(8,128)(2,1)S(1)}, bf16[2,512,256]{2,1,0:T(8,128)(2,1)S(1)}, u32[]{:S(2)}, u32[]{:S(2)}) collective-permute-start(bf16[2,512,256]{2,1,0:T(8,128)(2,1)S(1)} %pad_maximum_fusion.1.refs_5_), channel_id=1, source_target_pairs={{0,16},{16,0},{1,17},{17,1},{2,18},{18,2},{3,19},{19,3},{4,20},{20... | collective-permute-start | bytes 1572872 | tf_op jit(solution)/shard_map/ppermute | solution.py:374
  88.7 19.3 %collective-permute-start.25 = (bf16[2,512,256]{2,1,0:T(8,128)(2,1)S(1)}, bf16[2,512,256]{2,1,0:T(8,128)(2,1)S(1)}, u32[]{:S(2)}, u32[]{:S(2)}) collective-permute-start(bf16[2,512,256]{2,1,0:T(8,128)(2,1)S(1)} %pad_maximum_fusion.refs_4_), channel_id=1, source_target_pairs={{0,2},{2,0},{1,3},{3,1},{4,6},{6,4},{5,7},{7,5},{8,10},{10,8},{9,1... | collective-permute-start | bytes 1572872 | tf_op jit(solution)/shard_map/ppermute | solution.py:373
  98.1 21.0 %collective-permute-start.8 = (bf16[2,64,2048]{2,1,0:T(8,128)(2,1)S(1)}, bf16[2,64,2048]{2,1,0:T(8,128)(2,1)}, u32[]{:S(2)}, u32[]{:S(2)}) collective-permute-start(bf16[2,64,2048]{2,1,0:T(8,128)(2,1)S(1)} %broadcast_select_fusion.1.refs_2_), channel_id=1, source_target_pairs={{0,1},{1,0},{2,3},{3,2},{4,5},{5,4},{6,7},{7,6},{8,9},{9,8},{10,11... | collective-permute-start | bytes 1572872 | tf_op jit(solution)/shard_map/ppermute | solution.py:437
  98.8 20.8 %collective-permute-start.7 = (bf16[2,64,2048]{2,1,0:T(8,128)(2,1)S(1)}, bf16[2,64,2048]{2,1,0:T(8,128)(2,1)}, u32[]{:S(2)}, u32[]{:S(2)}) collective-permute-start(bf16[2,64,2048]{2,1,0:T(8,128)(2,1)S(1)} %broadcast_select_fusion.2.refs_1_), channel_id=1, source_target_pairs={{0,1},{1,0},{2,3},{3,2},{4,5},{5,4},{6,7},{7,6},{8,9},{9,8},{10,11... | collective-permute-start | bytes 1572872 | tf_op jit(solution)/shard_map/ppermute | solution.py:437
  100.1 21.0 %collective-permute-start.9 = (bf16[2,64,2048]{2,1,0:T(8,128)(2,1)S(1)}, bf16[2,64,2048]{2,1,0:T(8,128)(2,1)}, u32[]{:S(2)}, u32[]{:S(2)}) collective-permute-start(bf16[2,64,2048]{2,1,0:T(8,128)(2,1)S(1)} %broadcast_select_fusion.refs_3_), channel_id=1, source_target_pairs={{0,1},{1,0},{2,3},{3,2},{4,5},{5,4},{6,7},{7,6},{8,9},{9,8},{10,11... | collective-permute-start | bytes 1572872 | tf_op jit(solution)/shard_map/ppermute | solution.py:437
  116.0 24.2 %collective-permute-start.26 = (bf16[2,512,256]{2,1,0:T(8,128)(2,1)S(1)}, bf16[2,512,256]{2,1,0:T(8,128)(2,1)S(1)}, u32[]{:S(2)}, u32[]{:S(2)}) collective-permute-start(bf16[2,512,256]{2,1,0:T(8,128)(2,1)S(1)} %pad_maximum_fusion.1.refs_5_), channel_id=1, source_target_pairs={{0,2},{2,0},{1,3},{3,1},{4,6},{6,4},{5,7},{7,5},{8,10},{10,8},{9,1... | collective-permute-start | bytes 1572872 | tf_op jit(solution)/shard_map/ppermute | solution.py:376
  118.6 22.1 %collective-permute-start.27 = (bf16[2,512,256]{2,1,0:T(8,128)(2,1)S(1)}, bf16[2,512,256]{2,1,0:T(8,128)(2,1)S(1)}, u32[]{:S(2)}, u32[]{:S(2)}) collective-permute-start(bf16[2,512,256]{2,1,0:T(8,128)(2,1)S(1)} %pad_maximum_fusion.refs_4_), channel_id=1, source_target_pairs={{0,16},{16,0},{1,17},{17,1},{2,18},{18,2},{3,19},{19,3},{4,20},{20... | collective-permute-start | bytes 1572872 | tf_op jit(solution)/shard_map/ppermute | solution.py:375
  119.1 24.4 %collective-permute-start.30 = (bf16[2,512,256]{2,1,0:T(8,128)(2,1)}, bf16[2,512,256]{2,1,0:T(8,128)(2,1)S(1)}, u32[]{:S(2)}, u32[]{:S(2)}) collective-permute-start(bf16[2,512,256]{2,1,0:T(8,128)(2,1)} %copy-done.2), channel_id=1, source_target_pairs={{0,2},{2,0},{1,3},{3,1},{4,6},{6,4},{5,7},{7,5},{8,10},{10,8},{9,1... | collective-permute-start | bytes 1572872 | tf_op jit(solution)/shard_map/ppermute | solution.py:378
  119.6 23.9 %collective-permute-start.29 = (bf16[2,512,256]{2,1,0:T(8,128)(2,1)}, bf16[2,512,256]{2,1,0:T(8,128)(2,1)S(1)}, u32[]{:S(2)}, u32[]{:S(2)}) collective-permute-start(bf16[2,512,256]{2,1,0:T(8,128)(2,1)} %copy-done.4), channel_id=1, source_target_pairs={{0,16},{16,0},{1,17},{17,1},{2,18},{18,2},{3,19},{19,3},{4,20},{20... | collective-permute-start | bytes 1572872 | tf_op jit(solution)/shard_map/ppermute | solution.py:377
  (30 other events, 292.1 us)
